TPU v7x, 128 devices: a whole 4x4x4 slice. The times are simulated.
128 devices in a mesh: sp: 16 (over z, x), tp: 8 (over y, core).
Axes of the slice: x: 4, y: 4, z: 4, core: 2. Of those that a mesh axis runs over, the one named last changes fastest.
Arguments:
- target: bfloat16 [8192, 4096], P(('sp', 'tp')), may hold values from -0.07 to 0.07
- source: bfloat16 [16384, 4096], P(('sp', 'tp')), may hold values from -0.035 to 0.035
- gain_target: float32 [4096], replicated, may hold values from 0.1 to 1.9
- gain_source: float32 [4096], replicated, may hold values from 0.1 to 1.9
- w_query: bfloat16 [4096, 1024], P(None, 'tp'), may hold values from -1 to 1
- w_key: bfloat16 [4096, 512], replicated, may hold values from -1 to 1
- w_value: bfloat16 [4096, 512], replicated, may hold values from -0.09375 to 0.09375
- w_out: bfloat16 [1024, 4096], P('tp'), may hold values from -0.1875 to 0.1875
- grad_output: bfloat16 [8192, 4096], P(('sp', 'tp')), may hold values from -6 to 6
Outputs:
- grad_target: float32 [8192, 4096], P(('sp', 'tp'))
- grad_source: float32 [16384, 4096], P(('sp', 'tp'))
- grad_out_proj: float32 [1024, 4096], P('tp')
All inputs are finite; a program needn't handle non-finite values.
Results may differ from a plain program's by a relative error of at most 0.028.
Values may be sent and summed in bfloat16 or wider, within the bound.
A program may use at most 128 MiB of HBM per device.

v0:
```python
import math

import jax
import jax.numpy as jnp
from jax import lax
from jax.sharding import PartitionSpec as P

HD = 64


EPS = 1e-06


def sent_together(arrays, axis, dim, along):
    both = jnp.concatenate(arrays, axis=along)
    whole, at, finished = (lax.all_gather(both, axis, axis=dim, tiled=True), 0, [])
    for a in arrays:
        finished.append(lax.slice_in_dim(whole, at, at + a.shape[along], axis=along))
        at += a.shape[along]
    return tuple(finished)


def normalize(matrix, scaling):
    widened = matrix.astype(jnp.float32)
    factor = lax.rsqrt(jnp.mean(widened * widened, axis=-1, keepdims=True) + EPS)
    return (widened * factor * scaling).astype(jnp.bfloat16)


def norm_back(matrix, scaling, upstream):
    widened = matrix.astype(jnp.float32)
    factor = lax.rsqrt(jnp.mean(widened * widened, axis=-1, keepdims=True) + EPS)
    weighted = upstream * scaling
    inner = jnp.mean(widened * weighted, axis=-1, keepdims=True)
    return factor * weighted - widened * factor * factor * factor * inner


def score_block(queries, key_block, score_scale):
    return (
        jnp.einsum(
            "tkgd,skd->kgts", queries, key_block[:, :, 0], preferred_element_type=jnp.float32
        )
        * score_scale
    )


def split_arrived(arrived, key_count):
    row_count = arrived.shape[0]
    block_size = math.gcd(row_count, 1024)
    return (arrived.reshape(row_count // block_size, block_size, key_count, 2, HD), block_size)


def shards(target, source, gain_target, gain_source, w_query, w_key, w_value, w_out, grad_output):
    contract_last = (((1,), (1,)), ((), ()))
    across = lax.axis_size("tp")
    heads_all = w_key.shape[1] // HD
    key_count = heads_all // across
    query_count = w_query.shape[1] // HD
    group_size = query_count // key_count
    score_scale = float(HD) ** (-0.5)
    normed_target = normalize(target, gain_target)
    normed_source = normalize(source, gain_source)
    gathered_target, gathered_grad = sent_together((normed_target, grad_output), "tp", 0, 1)
    query = jnp.dot(gathered_target, w_query, preferred_element_type=jnp.float32).astype(
        jnp.bfloat16
    )
    head_grads = lax.dot_general(
        gathered_grad, w_out, contract_last, preferred_element_type=jnp.float32
    ).astype(jnp.bfloat16)
    row_count = query.shape[0]
    queries = query.reshape(row_count, key_count, group_size, HD)
    grad_heads = head_grads.reshape(row_count, key_count, group_size, HD)
    w_both = jnp.stack(
        [w_key.reshape(-1, heads_all, HD), w_value.reshape(-1, heads_all, HD)], axis=2
    )
    w_both = w_both.reshape(w_key.shape[0], heads_all * 2 * HD)
    pairs = jnp.dot(normed_source, w_both, preferred_element_type=jnp.float32).astype(jnp.bfloat16)
    own_pairs = lax.all_to_all(pairs, "tp", split_axis=1, concat_axis=0, tiled=True)
    start_max = jnp.full((key_count, group_size, row_count), -jnp.inf, jnp.float32)
    start_sum = jnp.zeros((key_count, group_size, row_count), jnp.float32)
    start_acc = jnp.zeros((row_count, key_count, group_size, HD), jnp.float32)
    blocks, block_size = split_arrived(
        lax.all_gather(own_pairs, "sp", axis=0, tiled=True), key_count
    )

    def absorb_advance(status, key_block):
        maxima, totals, accum = status
        scores = score_block(queries, key_block, score_scale)
        new_max = jnp.maximum(maxima, jnp.max(scores, axis=-1))
        shrink = jnp.exp(maxima - new_max)
        weights = jnp.exp(scores - new_max[..., None])
        totals = totals * shrink + jnp.sum(weights, axis=-1)
        partial_value = jnp.einsum(
            "kgts,skd->tkgd",
            weights.astype(jnp.bfloat16),
            key_block[:, :, 1],
            preferred_element_type=jnp.float32,
        )
        accum = accum * jnp.transpose(shrink, (2, 0, 1))[..., None] + partial_value
        return ((new_max, totals, accum), None)

    result, _ = lax.scan(absorb_advance, (start_max, start_sum, start_acc), blocks)
    maxima, totals, accum = result
    attn_heads = (accum / jnp.transpose(totals, (2, 0, 1))[..., None]).astype(jnp.bfloat16)
    delta_sum = jnp.sum(grad_heads.astype(jnp.float32) * attn_heads.astype(jnp.float32), axis=-1)
    delta_sum = jnp.transpose(delta_sum, (1, 2, 0))
    all_rows = own_pairs.shape[0] * lax.axis_size("sp")
    start_grad = jnp.zeros((row_count, key_count, group_size, HD), jnp.float32)
    start_pairs = jnp.zeros((all_rows, key_count * 2 * HD), jnp.float32)
    blocks, block_size = split_arrived(
        lax.all_gather(own_pairs, "sp", axis=0, tiled=True), key_count
    )

    def collect_advance(status, bundle):
        query_grad, pair_store = status
        key_block, position = bundle
        scores = score_block(queries, key_block, score_scale)
        attend = jnp.exp(scores - maxima[..., None]) / totals[..., None]
        grad_attend = jnp.einsum(
            "tkgd,skd->kgts", grad_heads, key_block[:, :, 1], preferred_element_type=jnp.float32
        )
        mixed = (attend * (grad_attend - delta_sum[..., None]) * score_scale).astype(jnp.bfloat16)
        query_grad = query_grad + jnp.einsum(
            "kgts,skd->tkgd", mixed, key_block[:, :, 0], preferred_element_type=jnp.float32
        )
        grad_key = jnp.einsum("kgts,tkgd->skd", mixed, queries, preferred_element_type=jnp.float32)
        grad_value = jnp.einsum(
            "kgts,tkgd->skd",
            attend.astype(jnp.bfloat16),
            grad_heads,
            preferred_element_type=jnp.float32,
        )
        stacked = jnp.stack([grad_key, grad_value], axis=2).reshape(block_size, key_count * 2 * HD)
        where_rows = position * block_size
        pair_store = lax.dynamic_update_slice_in_dim(pair_store, stacked, where_rows, 0)
        return ((query_grad, pair_store), None)

    positions = jnp.arange(blocks.shape[0], dtype=jnp.int32)
    result, _ = lax.scan(collect_advance, (start_grad, start_pairs), (blocks, positions))
    query_grad, pair_store = result
    pair_grads = lax.psum_scatter(
        pair_store.astype(jnp.bfloat16), "sp", scatter_dimension=0, tiled=True
    )
    grad_query = query_grad.astype(jnp.bfloat16).reshape(row_count, query_count * HD)
    pair_rows = lax.all_to_all(pair_grads, "tp", split_axis=0, concat_axis=1, tiled=True)
    grad_sn = lax.dot_general(pair_rows, w_both, contract_last, preferred_element_type=jnp.float32)
    grad_source = norm_back(source, gain_source, grad_sn)
    attention = attn_heads.reshape(row_count, query_count * HD)
    proj_part = lax.dot_general(
        attention, gathered_grad, (((0,), (0,)), ((), ())), preferred_element_type=jnp.float32
    )
    grad_out_proj = lax.psum(proj_part.astype(jnp.bfloat16), "sp").astype(jnp.float32)
    grad_xn = lax.psum_scatter(
        lax.dot_general(
            grad_query, w_query, contract_last, preferred_element_type=jnp.float32
        ).astype(jnp.bfloat16),
        "tp",
        scatter_dimension=0,
        tiled=True,
    ).astype(jnp.float32)
    grad_target = norm_back(target, gain_target, grad_xn)
    return (grad_target, grad_source, grad_out_proj)


def solution(mesh):
    return jax.shard_map(
        shards,
        mesh=mesh,
        in_specs=(
            P(("sp", "tp"), None),
            P(("sp", "tp"), None),
            P(),
            P(),
            P(None, "tp"),
            P(),
            P(),
            P("tp", None),
            P(("sp", "tp"), None),
        ),
        out_specs=(P(("sp", "tp"), None), P(("sp", "tp"), None), P("tp", None)),
        check_vma=False,
    )
```

profile of v0, /device:TPU:1, one launch (start us, length us, event | category | flops | bytes accessed | tf_op | source)
XLA Modules:
  0.0 471.1 jit_solution(16521432054210177134)
XLA Ops:
  7.2 1.6 fusion.55
  8.8 6.5 %copy.31 = bf16[4096,512]{0,1:T(8,128)(2,1)} copy(bf16[4096,512]{1,0:T(8,128)(2,1)} %param.18) | data formatting | bytes 8388608 | tf_op args[5]
  15.3 6.4 %copy.32 = bf16[4096,512]{0,1:T(8,128)(2,1)} copy(bf16[4096,512]{1,0:T(8,128)(2,1)} %param.19) | data formatting | bytes 8388608 | tf_op args[6]
  21.7 7.4 %pad_maximum_fusion.1 = bf16[4096,8,2,64]{0,3,1,2:T(8,128)(2,1)} fusion(bf16[4096,8,1,64]{0,3,1,2:T(8,128)(2,1)} %bitcast.250, bf16[4096,8,1,64]{0,3,1,2:T(8,128)(2,1)} %bitcast.249), kind=kLoop, calls=%fused_computation.49 | loop fusion | flops 4194304 | bytes 16777216 | tf_op jit(solution)/shard_map/stack | solution.py:72
  29.1 7.8 %copy.33 = bf16[4096,8,2,64]{0,3,2,1:T(8,128)(2,1)} copy(bf16[4096,8,2,64]{0,3,1,2:T(8,128)(2,1)} %pad_maximum_fusion.1) | data formatting | bytes 16777216 | tf_op jit(solution)/shard_map/stack | solution.py:72
  37.0 6.4 %fusion.59 = bf16[16,8,8,128]{3,2,1,0:T(8,128)(2,1)S(1)} fusion(bf16[4096,1024]{0,1:T(8,128)(2,1)} %bitcast.246, bf16[128,4096]{1,0:T(8,128)(2,1)S(1)} %copy-done.1, f32[4096]{0:T(1024)S(1)} %copy-done.6, f32[128]{0:T(128)S(1)} %add_rsqrt_fusion), kind=kOutput, calls=%fused_computation.75 | convolution fusion | flops 1075970048 | bytes 9716224 | tf_op jit(solution)/shard_map/dot_general | solution.py:76
  43.4 12.3 %all_to_all.38 = bf16[128,8,128]{2,0,1:T(8,128)(2,1)} all-to-all(bf16[128,8,128]{2,0,1:T(8,128)(2,1)S(1)} %bitcast.259), channel_id=1, replica_groups=mesh['sp'=16,'tp'=8] {'tp'}, dimensions={1} | all-to-all | bytes 524288 | tf_op jit(solution)/shard_map/all_to_all | solution.py:77
  56.3 1.0 pad_maximum_fusion.2
  57.6 50.4 %all-gather.3.cloned.1.call-done = bf16[16384,128]{1,0:T(8,128)(2,1)} async-done(((bf16[1024,128]{1,0:T(8,128)(2,1)}), bf16[16384,128]{1,0:T(8,128)(2,1)}) %all-gather.3.cloned.1.call-update) | async-done | bytes 4194320 | tf_op jit(solution)/shard_map/all_gather | solution.py:110
  108.0 14.7 %reshape.168 = bf16[16,1024,1,2,64]{4,3,1,0,2:T(2,128)(2,1)} reshape(bf16[16384,128]{1,0:T(8,128)(2,1)} %all-gather.3.cloned.1.call-done) | data formatting | bytes 8388608 | tf_op jit(solution)/shard_map/reshape | solution.py:49
  122.7 20.2 %copy.37 = bf16[16,1024,1,2,64]{1,4,3,2,0:T(8,128)(2,1)} copy(bf16[16,1024,1,2,64]{4,3,1,0,2:T(2,128)(2,1)} %reshape.168) | data formatting | bytes 8388608
  142.9 17.2 %all-gather.5.cloned.1.call-done = bf16[512,8192]{1,0:T(8,128)(2,1)} async-done(((bf16[64,8192]{1,0:T(8,128)(2,1)}), bf16[512,8192]{1,0:T(8,128)(2,1)}) %all-gather.5.cloned.1.call-update) | async-done | bytes 8388624 | tf_op jit(solution)/shard_map/all_gather | solution.py:16
  160.1 3.7 fusion.63
  163.8 54.3 %while.28 = (s32[]{:T(128)}, f32[1,2,512]{2,1,0:T(2,128)S(1)}, f32[1,2,512]{2,1,0:T(2,128)S(1)}, f32[512,1,2,64]{0,3,2,1:T(8,128)S(1)}, bf16[16,1024,1,2,64]{1,4...) while((s32[]{:T(128)}, f32[1,2,512]{2,1,0:T(2,128)S(1)}, ...), condition=%wide.region_5.6_spmd.clone, body=%wide.region_2.5_spmd.clone.sunk | while | flops 277026816 | bytes 14090349 | solution.py:101
  163.8 1.0 dynamic-slice_bitcast_fusion.4
  167.2 1.0 dynamic-slice_bitcast_fusion.4
  170.6 1.0 dynamic-slice_bitcast_fusion.4
  174.0 1.0 dynamic-slice_bitcast_fusion.4
  177.4 1.0 dynamic-slice_bitcast_fusion.4
  180.8 1.0 dynamic-slice_bitcast_fusion.4
  184.2 1.0 dynamic-slice_bitcast_fusion.4
  187.6 1.0 dynamic-slice_bitcast_fusion.4
  191.0 1.0 dynamic-slice_bitcast_fusion.4
  194.4 1.0 dynamic-slice_bitcast_fusion.4
  197.8 1.0 dynamic-slice_bitcast_fusion.4
  201.1 1.0 dynamic-slice_bitcast_fusion.4
  204.5 1.0 dynamic-slice_bitcast_fusion.4
  207.9 1.0 dynamic-slice_bitcast_fusion.4
  211.3 1.0 dynamic-slice_bitcast_fusion.4
  214.7 1.0 dynamic-slice_bitcast_fusion.4
  218.1 4.0 fusion.60
  222.2 3.9 convolution_convert_fusion.1
  226.2 2.2 broadcast_in_dim.6.clone
  228.4 110.4 %while.29 = (s32[]{:T(128)}, f32[512,1,2,64]{0,3,2,1:T(8,128)S(1)}, bf16[16384,128]{1,0:T(8,128)(2,1)}, bf16[16,1024,1,2,64]{1,4,3,2,0:T(8,128)(2,1)}, bf16[512,...) while((s32[]{:T(128)}, f32[512,1,2,64]{0,3,2,1:T(8,128)S(1)}, ...), condition=%wide.region_8.9_spmd.clone, body=%wide.region_7.8_spmd.clone.sunk | while | flops 679739392 | bytes 22687960 | solution.py:138
  229.6 1.0 dynamic-slice_bitcast_fusion.5
  236.5 1.0 dynamic-slice_bitcast_fusion.5
  237.5 1.0 fusion.110
  243.4 1.0 dynamic-slice_bitcast_fusion.5
  250.3 1.0 dynamic-slice_bitcast_fusion.5
  257.2 1.0 dynamic-slice_bitcast_fusion.5
  264.1 1.0 dynamic-slice_bitcast_fusion.5
  270.9 1.0 dynamic-slice_bitcast_fusion.5
  271.9 1.0 fusion.110
  277.8 1.0 dynamic-slice_bitcast_fusion.5
  278.8 1.0 fusion.110
  284.7 1.0 dynamic-slice_bitcast_fusion.5
  291.6 1.0 dynamic-slice_bitcast_fusion.5
  292.6 1.0 fusion.110
  298.6 1.0 dynamic-slice_bitcast_fusion.5
  299.5 1.0 fusion.110
  305.5 1.0 dynamic-slice_bitcast_fusion.5
  312.4 1.0 dynamic-slice_bitcast_fusion.5
  319.3 1.0 dynamic-slice_bitcast_fusion.5
  326.2 1.0 dynamic-slice_bitcast_fusion.5
  333.1 1.0 dynamic-slice_bitcast_fusion.5
  338.9 3.3 convolution_convert_fusion
  342.2 2.8 convert_element_type.82
  345.0 70.6 %reduce-scatter.5.cloned.1.call-done = bf16[1024,128]{1,0:T(8,128)(2,1)} async-done(((bf16[16384,128]{1,0:T(8,128)(2,1)}), bf16[1024,128]{1,0:T(8,128)(2,1)}) %reduce-scatter.5.cloned.1.call-update) | async-done | bytes 262160 | tf_op jit(solution)/shard_map/reduce_scatter | solution.py:140
  415.6 6.7 %all-to-all-start.1 = ((bf16[8,128,128]{2,1,0:T(8,128)(2,1)}), bf16[8,128,128]{2,1,0:T(8,128)(2,1)S(1)}, u32[]{:S(2)}, u32[]{:S(2)}) async-start(bf16[8,128,128]{2,1,0:T(8,128)(2,1)} %bitcast.262), calls=%async_computation.3 | async-start | bytes 524288 | tf_op jit(solution)/shard_map/all_to_all | solution.py:144
  422.3 31.5 %reduce-scatter.3.cloned.1.call-done = bf16[64,4096]{1,0:T(8,128)(2,1)} async-done(((bf16[512,4096]{1,0:T(8,128)(2,1)}), bf16[64,4096]{1,0:T(8,128)(2,1)}) %reduce-scatter.3.cloned.1.call-update) | async-done | bytes 524304 | tf_op jit(solution)/shard_map/reduce_scatter | solution.py:152
  453.8 1.3 fusion.71
  455.1 2.4 fusion.69
  457.7 4.9 %fusion.56 = (f32[128]{0:T(128)S(1)}, f32[128,4096]{1,0:T(8,128)S(1)}) fusion(bf16[128,4096]{1,0:T(8,128)(2,1)S(1)} %copy-done.1, f32[4096]{0:T(1024)S(1)} %copy-done.6, bf16[128,1024]{0,1:T(8,128)(2,1)S(1)} %bitcast.256, bf16[4096,1024]{0,1:T(8,128)(2,1)} %bitcast.247), kind=kOutput, calls=%fused_computation.68 | convolution fusion | flops 1075838848 | bytes 11813376 | tf_op jit(solution)/shard_map/dot_general | solution.py:145
  462.6 1.9 fusion.54
  (276 shorter events, 117.9 us)
Async XLA Ops:
  7.2 152.9 %copy-start = (bf16[4096,128]{1,0:T(8,128)(2,1)S(1)}, bf16[4096,128]{1,0:T(8,128)(2,1)}, u32[]{:S(2)}) copy-start(bf16[4096,128]{1,0:T(8,128)(2,1)} %param.17) | copy-start | bytes 3145732
  7.2 100.8 %all-gather.3.cloned.1.call-start = ((), (), s32[]{:S(2)}) async-start(), calls=%async_computation.4 | async-start | bytes 4456448 | tf_op jit(solution)/shard_map/all_gather | solution.py:110
  29.1 7.8 %copy-start.1 = (bf16[128,4096]{1,0:T(8,128)(2,1)S(1)}, bf16[128,4096]{1,0:T(8,128)(2,1)}, u32[]{:S(2)}) copy-start(bf16[128,4096]{1,0:T(8,128)(2,1)} %param.14) | copy-start | bytes 3145732
  29.1 7.8 %copy-start.6 = (f32[4096]{0:T(1024)S(1)}, f32[4096]{0:T(1024)}, u32[]{:S(2)}) copy-start(f32[4096]{0:T(1024)} %param.16) | copy-start | bytes 49156
  36.9 18.9 %copy-start.2 = (bf16[64,4096]{1,0:T(8,128)(2,1)S(1)}, bf16[64,4096]{1,0:T(8,128)(2,1)}, u32[]{:S(2)}) copy-start(bf16[64,4096]{1,0:T(8,128)(2,1)} %param.13) | copy-start | bytes 1572868
  36.9 19.1 %copy-start.5 = (f32[4096]{0:T(1024)S(1)}, f32[4096]{0:T(1024)}, u32[]{:S(2)}) copy-start(f32[4096]{0:T(1024)} %param.15) | copy-start | bytes 49156
  36.9 19.3 %copy-start.4 = (bf16[64,4096]{1,0:T(8,128)(2,1)S(1)}, bf16[64,4096]{1,0:T(8,128)(2,1)}, u32[]{:S(2)}) copy-start(bf16[64,4096]{1,0:T(8,128)(2,1)} %param.21) | copy-start | bytes 1572868
  55.8 104.3 %all-gather.5.cloned.1.call-start = ((), (), s32[]{:S(2)}) async-start(), calls=%async_computation.5 | async-start | bytes 9437184 | tf_op jit(solution)/shard_map/all_gather | solution.py:16
  57.3 284.8 %all-reduce.2.cloned.1.call-start = ((), (), s32[]{:S(2)}) async-start(), calls=%async_computation.8 | async-start | bytes 2097152 | tf_op jit(solution)/shard_map/psum | solution.py:151
  226.1 189.5 %reduce-scatter.5.cloned.1.call-start = ((), (), s32[]{:S(2)}) async-start(), calls=%async_computation.7 | async-start | bytes 4456448 | tf_op jit(solution)/shard_map/reduce_scatter | solution.py:140
  338.8 115.0 %reduce-scatter.3.cloned.1.call-start = ((), (), s32[]{:S(2)}) async-start(), calls=%async_computation.6 | async-start | bytes 4718592 | tf_op jit(solution)/shard_map/reduce_scatter | solution.py:152
  342.1 111.7 %copy-start.3 = (bf16[64,4096]{1,0:T(8,128)(2,1)S(1)}, bf16[64,4096]{1,0:T(8,128)(2,1)}, u32[]{:S(2)}) copy-start(bf16[64,4096]{1,0:T(8,128)(2,1)} %param.13) | copy-start | bytes 1572868
  415.6 41.9 %all-to-all-start.1 = ((bf16[8,128,128]{2,1,0:T(8,128)(2,1)}), bf16[8,128,128]{2,1,0:T(8,128)(2,1)S(1)}, u32[]{:S(2)}, u32[]{:S(2)}) async-start(bf16[8,128,128]{2,1,0:T(8,128)(2,1)} %bitcast.262), calls=%async_computation.3 | async-start | bytes 524288 | tf_op jit(solution)/shard_map/all_to_all | solution.py:144
Sparse Core Ops, SparseCore 0:
  55.9 52.0 all-gather.2
  110.2 49.8 all-gather.4
  226.2 85.7 all-reduce.1
  338.9 76.6 reduce-scatter.4
  417.9 35.8 reduce-scatter.2
where the time goes:
time: 476 us; the launch traced here: 471 us
  waiting for transfers between devices  170 us (36%)
  local copies, waits for them, and re-layouts  113 us (24%)
  matrix products  112 us (24%)
  other arithmetic  31.2 us (7%)
  between operations  14 us (3%)
  blocking collectives  12.3 us (3%)
  loops' own time  12 us (3%)
  starting transfers between devices  7.12 us (1%)
    reduce_scatter x1, waiting for transfers between devices, shards(): lax.psum_scatter(pair_store.astype(jnp.bfloat16), 'sp', scatter_dimension...  70.6 us
    all_gather x1, waiting for transfers between devices, shards(): lax.all_gather(own_pairs, 'sp', axis=0, tiled=True)  50.4 us
    unnamed x17, local copies, waits for them, and re-layouts  33.1 us
    reduce_scatter x1, waiting for transfers between devices, shards(): lax.psum_scatter(lax.dot_general(grad_query, w_query, contract_last, pref...  31.5 us
    squeeze x32, local copies, waits for them, and re-layouts, shards(): lax.scan(absorb_advance, (start_max, start_sum, start_acc), blocks)  31.2 us
    dot_general x32, matrix products, score_block(): jnp.einsum('tkgd,skd->kgts', queries, key_block[:, :, 0], preferred_eleme...  27.2 us
    all_gather x1, waiting for transfers between devices, sent_together(): lax.all_gather(both, axis, axis=dim, tiled=True)  17.2 us
    reshape x1, local copies, waits for them, and re-layouts, split_arrived(): arrived.reshape(row_count // block_size, block_size, key_count, 2, HD)  14.7 us
  transfers between devices with their start and end apart: 6, of which 4 were waited for; matrix products, arithmetic and copies ran while one was open for 31% of the time, Pallas kernels for 0%

commit v1 on v0

v1 whole, which is shorter than its diff:
```python
import functools

import jax
import jax.numpy as jnp
from jax import lax
from jax.experimental import pallas as pl
from jax.experimental.pallas import tpu as pltpu
from jax.sharding import PartitionSpec as P

BF = jnp.bfloat16
F32 = jnp.float32
EPS = 1e-06
MESH = pl.DeviceIdType.MESH

T = 512
TT = 2 * T
U = 1024
XN0 = 4096


def dot(a, b):
    return jnp.dot(a, b, preferred_element_type=F32)


def dot_t(a, b):
    return lax.dot_general(a, b, (((1,), (1,)), ((), ())), preferred_element_type=F32)


def normalize(rows, gain):
    wide = rows.astype(F32)
    factor = lax.rsqrt(jnp.mean(wide * wide, axis=-1, keepdims=True) + EPS)
    return (wide * factor * gain).astype(BF)


def order(i):
    return i + i // 2 - 2 * (i // 3)


class Coords:
    def __init__(self):
        self.sp = lax.axis_index("sp")
        self.tp = lax.axis_index("tp")
        self.z, self.x = self.sp // 4, self.sp % 4
        self.y, self.c = self.tp // 2, self.tp % 2

    def block(self, half, a, b):
        if half == 0:
            return ((self.z + b) % 4) * 4 + (self.x + a) % 4
        return ((self.z + a) % 4) * 4 + (self.x + b) % 4

    def ring(self, d, sib):
        return ((self.y + d) % 4) * 2 + (self.c if sib == 0 else 1 - self.c)


class Net:
    def __init__(self, at, send_sems, stand_in):
        self.at, self.sems, self.count, self.stand_in = at, send_sems, 0, stand_in

    def push(self, src, dst, recv, sp=None, tp=None):
        number = self.count
        sem = self.sems.at[number]
        self.count += 1
        who = (self.at.sp if sp is None else sp, self.at.tp if tp is None else tp)
        copy = pltpu.make_async_remote_copy(
            src_ref=src, dst_ref=dst, send_sem=sem, recv_sem=recv, device_id=who, device_id_type=MESH
        )
        copy.start()
        return number, src.shape

    def sent(self, copies):
        for number, (rows, columns) in copies:
            place = self.stand_in.at[pl.ds(0, rows), pl.ds(0, columns)]
            pltpu.make_async_remote_copy(
                src_ref=place, dst_ref=place, send_sem=self.sems.at[number], recv_sem=self.sems.at[number],
                device_id=(self.at.sp, self.at.ring(1, 0)), device_id_type=MESH,
            ).wait_send()

    def arrive(self, dst, recv):
        pltpu.make_async_remote_copy(
            src_ref=dst, dst_ref=dst, send_sem=self.sems.at[0], recv_sem=recv,
            device_id=(self.at.sp, self.at.ring(1, 0)), device_id_type=MESH,
        ).wait_recv()


class RowsGather:
    def __init__(self, net, place, recv):
        self.net, self.place, self.recv = net, place, recv

    def send(self, d, h, way):
        at = self.net.at
        src = self.place(at.ring(d, 0), h)
        if way == 0:
            return self.net.push(src, src, self.recv.at[d, 1, h], tp=at.ring(0, 1))
        return self.net.push(src, src, self.recv.at[(d - way) % 4, 0, h], tp=at.ring(way, 0))

    def begin(self):
        s = self.send
        return [s(0, 0, 1), s(0, 1, -1), s(0, 1, 1), s(0, 0, -1), s(0, 0, 0), s(0, 1, 0)]

    def come(self, d, h, sib):
        at = self.net.at
        self.net.arrive(self.place(at.ring(d, sib), h), self.recv.at[d, sib, h])
        sent = []
        if sib == 0:
            if (d, h) == (3, 0):
                sent.append(self.send(d, h, 1))
            if (d, h) == (1, 1):
                sent.append(self.send(d, h, -1))
            sent.append(self.send(d, h, 0))
        return sent


FIRST = [(3, 0), (1, 1)]
SECOND = [(3, 1), (1, 0), (2, 0), (2, 1)]
SIBS = [(0, 0), (0, 1), (3, 0), (1, 1), (3, 1), (1, 0), (2, 0), (2, 1)]


class PairsGather:
    def __init__(self, net, kv, recv):
        self.net, self.kv, self.recv = net, kv, recv

    def rows(self, half, a, b, piece):
        start = self.net.at.block(half, a, b) * 1024 + half * 512 + piece * 256
        return self.kv.at[pl.ds(pl.multiple_of(start, 256), 256), :]

    def send(self, half, a, b, piece, axis, way):
        at = self.net.at
        src = self.rows(half, a, b, piece)
        if axis == 0:
            to, a2, b2 = at.block(half, way, 0), (a - way) % 4, b
        else:
            to, a2, b2 = at.block(half, 0, way), a, (b - way) % 4
        return self.net.push(src, src, self.recv.at[half, a2, b2, piece], sp=to)

    def begin(self):
        sent = []
        for piece, way in ((0, 1), (1, -1), (1, 1), (0, -1)):
            for half in (0, 1):
                sent.append(self.send(half, 0, 0, piece, 0, way))
        for piece, way in ((0, 1), (1, -1), (1, 1), (0, -1)):
            for half in (0, 1):
                sent.append(self.send(half, 0, 0, piece, 1, way))
        return sent

    def come(self, a, b, piece):
        sent = []
        for half in (0, 1):
            self.net.arrive(self.rows(half, a, b, piece), self.recv.at[half, a, b, piece])
            if b == 0:
                if (a, piece) == (3, 0):
                    sent.append(self.send(half, a, b, piece, 0, 1))
                if (a, piece) == (1, 1):
                    sent.append(self.send(half, a, b, piece, 0, -1))
                for way in (1, -1):
                    sent.append(self.send(half, a, b, piece, 1, way))
            else:
                if (b, piece) == (3, 0):
                    sent.append(self.send(half, a, b, piece, 1, 1))
                if (b, piece) == (1, 1):
                    sent.append(self.send(half, a, b, piece, 1, -1))
        return sent


PHASE1 = [(3, 0, 0), (1, 0, 1), (3, 0, 1), (1, 0, 0), (2, 0, 0), (2, 0, 1)]
PHASE2 = (
    [(0, 3, 0), (0, 1, 1), (0, 3, 1), (0, 1, 0)]
    + [e for a in (3, 1) for e in ((a, 3, 0), (a, 1, 1), (a, 3, 1), (a, 1, 0))]
    + [(0, 2, 0), (0, 2, 1)]
    + [(2, 3, 0), (2, 1, 1), (2, 3, 1), (2, 1, 0)]
    + [e for a in (3, 1, 2) for e in ((a, 2, 0), (a, 2, 1))]
)


def kernel(
    tgt, src, gain_t, gain_s, wq, wk, wv, wo, go,
    wq_all, gop, dq_loc, dkv_loc,
    E, kv, gg, dkv, hop, end1, hop2, end2, ar1, ar2,
    qT, qP, dT, dP, acc, m_run, m_unit, dqT, oT, pr, back, fin, dqs,
    tgt_v, wo_v, gt_v, gs_v,
    send_sems, load_sems, r_xn, r_gg, r_wq, r_a2a, r_kv, r_rs1, r_rs2, r_rs3, r_rs4, r_ar, r_dq, r_dkv,
):
    src_v = gop
    arP = wo_v
    at = Coords()
    net = Net(at, send_sems, E)
    lane = lax.broadcasted_iota(jnp.int32, (1, 128), 1)
    low = lane < 64

    barrier = pltpu.get_barrier_semaphore()
    others = [(at.sp, (at.tp + j) % 8) for j in range(1, 8)]
    others += [(at.block(0, a, 0), at.tp) for a in (1, 2, 3)]
    others += [(at.block(0, 0, b), at.tp) for b in (1, 2, 3)]
    for who in others:
        pl.semaphore_signal(barrier, inc=1, device_id=who, device_id_type=MESH)

    gg_own = [
        pltpu.make_async_copy(
            go.at[:, pl.ds(1024 * k, 1024)],
            gg.at[pl.ds(pl.multiple_of(at.tp * 256 + 64 * k, 64), 64), :],
            load_sems.at[8 + k],
        )
        for k in range(4)
    ]
    loads = [
        pltpu.make_async_copy(tgt, tgt_v, load_sems.at[0]),
        pltpu.make_async_copy(gain_t, gt_v, load_sems.at[1]),
        pltpu.make_async_copy(src, src_v, load_sems.at[2]),
        pltpu.make_async_copy(gain_s, gs_v, load_sems.at[3]),
        pltpu.make_async_copy(wk, E.at[pl.ds(0, 4096), pl.ds(0, 512)], load_sems.at[4]),
        pltpu.make_async_copy(wv, E.at[pl.ds(0, 4096), pl.ds(512, 512)], load_sems.at[5]),
        pltpu.make_async_copy(wo, wo_v, load_sems.at[6]),
    ]
    loads_w = [
        pltpu.make_async_copy(
            wq.at[pl.ds(512 * k, 512), :], dkv.at[0, k // 4, k % 4], load_sems.at[16 + k]
        )
        for k in range(8)
    ]
    for load in loads + loads_w + gg_own:
        load.start()

    def xn_place(j, h):
        return E.at[pl.ds(pl.multiple_of(XN0 + j * 256 + h * 128, 128), 128), :]

    def gg_place(j, h):
        return gg.at[pl.ds(pl.multiple_of(j * 256 + h * 128, 128), 128), :]

    def wq_place(j, h):
        return wq_all.at[j, pl.ds(h * 2048, 2048), :]

    rows_x = RowsGather(net, xn_place, r_xn)
    rows_g = RowsGather(net, gg_place, r_gg)
    rows_w = RowsGather(net, wq_place, r_wq)

    loads[0].wait()
    loads[1].wait()
    xn = normalize(tgt_v[...], gt_v[...])
    for k in range(4):
        E[pl.ds(pl.multiple_of(XN0 + at.tp * 256 + 64 * k, 64), 64), :] = xn[:, 1024 * k : 1024 * k + 1024]
    pl.semaphore_wait(barrier, len(others))
    sent_x = rows_x.begin()

    loads[2].wait()
    loads[3].wait()
    sn = normalize(src_v[...], gs_v[...])
    loads[4].wait()
    loads[5].wait()
    pairs = dot(sn, E[0:4096, :])
    for g in range(4):
        kb = pairs[:, 128 * g : 128 * g + 128]
        vb = pairs[:, 512 + 128 * g : 512 + 128 * g + 128]
        pr[2 * g] = jnp.where(low, kb, pltpu.roll(vb, 64, 1)).astype(BF)
        pr[2 * g + 1] = jnp.where(low, pltpu.roll(kb, 64, 1), vb).astype(BF)
    mine = kv.at[pl.ds(pl.multiple_of(at.sp * 1024 + at.tp * 128, 128), 128), :]
    sent = []
    for j in (4, 3, 5, 2, 6, 1, 7):
        to = (at.tp + j) % 8
        sent.append(net.push(pr.at[to], mine, r_a2a.at[8 - j], tp=to))
    mine[...] = pr[at.tp]
    for j in range(1, 8):
        frm = (at.tp + j) % 8
        net.arrive(kv.at[pl.ds(pl.multiple_of(at.sp * 1024 + frm * 128, 128), 128), :], r_a2a.at[j])
    pairs_g = PairsGather(net, kv, r_kv)
    sent += pairs_g.begin()
    for load in gg_own:
        load.wait()
    loads[6].wait()
    for load in loads_w:
        load.wait()
    own_w = [
        pltpu.make_async_copy(
            dkv.at[0, k // 4, k % 4], wq_all.at[at.tp, pl.ds(512 * k, 512), :], load_sems.at[24 + k]
        )
        for k in range(8)
    ]
    for copy in own_w:
        copy.start()

    for d, h in FIRST:
        sent_x += rows_x.come(d, h, 0)
    sent += rows_g.begin()
    for e in PHASE1:
        sent += pairs_g.come(*e)
    for d, h in SECOND:
        sent_x += rows_x.come(d, h, 0)
    for e in PHASE2:
        sent += pairs_g.come(*e)
    for d, h in SIBS:
        rows_x.come(d, h, 1)

    def gathered(ref, base, k):
        return jnp.concatenate(
            [ref[base + j * 256 + k * 64 : base + j * 256 + k * 64 + 64, :] for j in range(8)], axis=0
        )

    def wq_rows(k):
        return jnp.concatenate([dkv[0, k // 2, 2 * (k % 2)], dkv[0, k // 2, 2 * (k % 2) + 1]], axis=0)

    q = dot(gathered(E, XN0, 0), wq_rows(0))
    for k in range(1, 4):
        q += dot(gathered(E, XN0, k), wq_rows(k))
    q = q.astype(BF).astype(F32)
    net.sent(sent_x)

    for d, h in FIRST:
        sent += rows_g.come(d, h, 0)
    for copy in own_w:
        copy.wait()
    sent += rows_w.begin()
    for d, h in SECOND:
        sent += rows_g.come(d, h, 0)
    for d, h in SIBS:
        rows_g.come(d, h, 1)
    do = dot_t(gathered(gg, 0, 0), wo_v[:, 0:1024])
    for k in range(1, 4):
        do += dot_t(gathered(gg, 0, k), wo_v[:, 1024 * k : 1024 * k + 1024])
    do = do.astype(BF).astype(F32)

    q0 = jnp.where(low, q, 0.0)
    q1 = jnp.where(low, pltpu.roll(q, 64, 1), 0.0)
    d0 = jnp.where(low, 0.0, pltpu.roll(do, 64, 1))
    d1 = jnp.where(low, 0.0, do)
    for h, (a, b) in enumerate(((q0, d0), (q1, d1))):
        r = slice(h * T, h * T + T)
        qP[r, :] = a.astype(BF)
        dP[r, :] = b.astype(BF)
        qT[:, r] = (a * 0.125).T.astype(BF)
        dT[:, r] = (b * 0.125).T.astype(BF)

    acc[...] = jnp.zeros_like(acc)
    m_run[...] = jnp.full_like(m_run, -jnp.inf)
    dqT[...] = jnp.zeros_like(dqT)
    ones = jnp.ones((16, U), BF)

    def unit_kv(a, b):
        parts = []
        for half in (0, 1):
            start = pl.multiple_of(at.block(half, a, b) * 1024 + half * 512, 512)
            parts.append(kv[pl.ds(start, 512), :])
        return jnp.concatenate(parts, axis=0)

    def fwd(u, _):
        block = unit_kv(order(u % 4), order(u // 4))
        s = dot(block, qT[...])
        m_old = m_run[...]
        m_new = jnp.maximum(m_old, jnp.max(s, axis=0, keepdims=True))
        shrink = jnp.exp(m_old - m_new)
        e = jnp.exp(s - m_new).astype(BF)
        E[pl.ds(pl.multiple_of(u * U, U), U), :] = e
        m_run[...] = m_new
        m_unit[pl.ds(u, 1)] = m_new[None]
        vt = block.astype(F32).T.astype(BF)[64:128, :]
        acc[...] = acc[...] * shrink + dot(jnp.concatenate([vt, ones], axis=0), e)
        return 0

    lax.fori_loop(0, 16, fwd, 0)
    inv = 1.0 / acc[64:65, :]
    o = (acc[0:64, :] * inv).astype(BF)
    oT[0:64, :] = o[:, 0:T]
    oT[64:128, :] = o[:, T:]
    delta = jnp.sum(dT[64:128, :].astype(F32) * o.astype(F32), axis=0, keepdims=True)
    m_end = m_run[...]

    for k in range(4):
        arP[:, 1024 * k : 1024 * k + 1024] = dot(oT[...], gathered(gg, 0, k)).astype(BF)

    def wide_col(half, a):
        pi = at.x if half == 0 else at.z
        return pl.ds(pl.multiple_of(half * 2048 + ((pi + a) % 4) * 512, 512), 512)

    def slim_col(half, b):
        pi, qi = (at.x, at.z) if half == 0 else (at.z, at.x)
        return pl.ds(pl.multiple_of(half * 2048 + pi * 512 + ((qi + b) % 4) * 128, 128), 128)

    def ar_1():
        for half in (0, 1):
            for a in (1, 3, 2):
                sent.append(net.push(arP.at[:, wide_col(half, a)], ar1.at[half, 4 - a], r_ar.at[0, half, 4 - a], sp=at.block(half, a, 0)))

    def ar_2():
        for half in (0, 1):
            total = arP[:, wide_col(half, 0)].astype(F32)
            for a in (1, 2, 3):
                net.arrive(ar1.at[half, a], r_ar.at[0, half, a])
                total += ar1[half, a].astype(F32)
            arP[:, wide_col(half, 0)] = total.astype(BF)
            for b in (1, 3, 2):
                sent.append(net.push(arP.at[:, slim_col(half, b)], ar2.at[half, 4 - b], r_ar.at[1, half, 4 - b], sp=at.block(half, 0, b)))

    def ar_3():
        for half in (0, 1):
            total = arP[:, slim_col(half, 0)].astype(F32)
            for b in (1, 2, 3):
                net.arrive(ar2.at[half, b], r_ar.at[1, half, b])
                total += ar2[half, b].astype(F32)
            gop[:, slim_col(half, 0)] = total.astype(BF)
            for b in (1, 3, 2):
                place = gop.at[:, slim_col(half, 0)]
                sent.append(net.push(place, place, r_ar.at[2, half, 4 - b], sp=at.block(half, 0, b)))

    def ar_4():
        for half in (0, 1):
            for b in (1, 2, 3):
                net.arrive(gop.at[:, slim_col(half, b)], r_ar.at[2, half, b])
            for a in (1, 3, 2):
                place = gop.at[:, wide_col(half, 0)]
                sent.append(net.push(place, place, r_ar.at[3, half, 4 - a], sp=at.block(half, a, 0)))

    def ar_5():
        for half in (0, 1):
            for a in (1, 2, 3):
                net.arrive(gop.at[:, wide_col(half, a)], r_ar.at[3, half, a])

    def add_to(place, arrived):
        place[...] = (place[...].astype(F32) + arrived[...].astype(F32)).astype(BF)

    def after(i):
        a, b = [2, 3, 1, 0][i // 4], [2, 3, 1, 0][i % 4]
        for half in (0, 1):
            piece = dkv.at[half, a, b]
            top, bottom = piece.at[pl.ds(0, 256), :], piece.at[pl.ds(256, 256), :]
            plus, minus = at.block(half, 1, 0), at.block(half, 3, 0)
            plus2, minus2 = at.block(half, 0, 1), at.block(half, 0, 3)
            if a == 2:
                sent.append(net.push(top, hop.at[half, 0, b], r_rs1.at[half, 0, b], sp=plus))
                sent.append(net.push(bottom, hop.at[half, 1, b], r_rs1.at[half, 1, b], sp=minus))
            elif a == 3:
                net.arrive(hop.at[half, 1, b], r_rs1.at[half, 1, b])
                add_to(bottom, hop.at[half, 1, b])
                sent.append(net.push(piece, end1.at[half, 1, b], r_rs2.at[half, 1, b], sp=minus))
            elif a == 1:
                net.arrive(hop.at[half, 0, b], r_rs1.at[half, 0, b])
                add_to(top, hop.at[half, 0, b])
                sent.append(net.push(piece, end1.at[half, 0, b], r_rs2.at[half, 0, b], sp=plus))
            else:
                total = piece[...].astype(F32)
                for side in (0, 1):
                    net.arrive(end1.at[half, side, b], r_rs2.at[half, side, b])
                    total += end1[half, side, b].astype(F32)
                if b == 2:
                    piece[...] = total.astype(BF)
                    sent.append(net.push(top, hop2.at[half, 0], r_rs3.at[half, 0], sp=plus2))
                    sent.append(net.push(bottom, hop2.at[half, 1], r_rs3.at[half, 1], sp=minus2))
                elif b == 3:
                    piece[...] = total.astype(BF)
                    net.arrive(hop2.at[half, 1], r_rs3.at[half, 1])
                    add_to(bottom, hop2.at[half, 1])
                    sent.append(net.push(piece, end2.at[half, 1], r_rs4.at[half, 1], sp=minus2))
                elif b == 1:
                    piece[...] = total.astype(BF)
                    net.arrive(hop2.at[half, 0], r_rs3.at[half, 0])
                    add_to(top, hop2.at[half, 0])
                    sent.append(net.push(piece, end2.at[half, 0], r_rs4.at[half, 0], sp=plus2))
                else:
                    for side in (0, 1):
                        net.arrive(end2.at[half, side], r_rs4.at[half, side])
                        total += end2[half, side].astype(F32)
                    fin[half * 512 : half * 512 + 512, :] = total.astype(BF)

    def bwd(i, _):
        for k in range(16):
            if k == 3:
                extra = [ar_2]
            elif k == 6:
                extra = [ar_3]
            elif k == 8:
                extra = [ar_4]
            else:
                extra = []

            @pl.when(i == k)
            def _(k=k, extra=extra):
                for f in extra:
                    f()
                if k > 0:
                    after(k - 1)
                if k == 2:
                    for d, h in FIRST:
                        sent.extend(rows_w.come(d, h, 0))
                if k == 9:
                    for d, h in SECOND:
                        sent.extend(rows_w.come(d, h, 0))

        ia, ib = 3 - i // 4, 3 - i % 4
        a, b = order(ia), order(ib)
        block = unit_kv(a, b)
        dp = dot(block, dT[...])
        u = ib * 4 + ia
        scale = jnp.exp(m_unit[u] - m_end) * inv
        p = E[pl.ds(pl.multiple_of(u * U, U), U), :].astype(F32) * scale
        g = (p * (dp - delta)).astype(BF)
        both = dot(g, qP[...]) + dot(p.astype(BF), dP[...])
        both = both.astype(BF)
        dkv[0, a, b] = both[0:512, :]
        dkv[1, a, b] = both[512:1024, :]
        kt = block.astype(F32).T.astype(BF)[0:64, :]
        dqT[...] += dot(kt, g)
        return 0

    ar_1()
    lax.fori_loop(0, 16, bwd, 0)

    grad = dqT[...]
    grad = jnp.concatenate([grad[:, 0:T], grad[:, T:]], axis=0).T.astype(BF)
    dqs[...] = grad
    for j in (4, 3, 5, 2, 6, 1, 7):
        to = (at.tp + j) % 8
        sent.append(net.push(
            dqs.at[pl.ds(pl.multiple_of(to * 64, 64), 64), :],
            dq_loc.at[at.tp], r_dq.at[8 - j], tp=to,
        ))
    dq_loc[at.tp] = dqs[pl.ds(pl.multiple_of(at.tp * 64, 64), 64), :]
    after(15)
    for j in (4, 3, 5, 2, 6, 1, 7):
        to = (at.tp + j) % 8
        sent.append(net.push(
            fin.at[pl.ds(pl.multiple_of(to * 128, 128), 128), :],
            back.at[at.tp], r_dkv.at[8 - j], tp=to,
        ))
    back[at.tp] = fin[pl.ds(pl.multiple_of(at.tp * 128, 128), 128), :]
    ar_5()
    for d, h in SIBS:
        rows_w.come(d, h, 1)
    for j in range(1, 8):
        frm = (at.tp + j) % 8
        net.arrive(dq_loc.at[frm], r_dq.at[j])
    for j in range(1, 8):
        frm = (at.tp + j) % 8
        net.arrive(back.at[frm], r_dkv.at[j])
    for g in range(4):
        even, odd = back[2 * g].astype(F32), back[2 * g + 1].astype(F32)
        dkv_loc[:, 128 * g : 128 * g + 128] = jnp.where(low, even, pltpu.roll(odd, 64, 1)).astype(BF)
        dkv_loc[:, 512 + 128 * g : 640 + 128 * g] = jnp.where(low, pltpu.roll(even, 64, 1), odd).astype(BF)
    net.sent(sent)


def mega(target, source, gain_t, gain_s, wq, wk, wv, wo, go):
    any_ = pl.BlockSpec(memory_space=pl.ANY)
    vmem = pl.BlockSpec(memory_space=pltpu.VMEM)
    V, D, S = pltpu.VMEM, pltpu.SemaphoreType.DMA, jax.ShapeDtypeStruct
    return pl.pallas_call(
        kernel,
        out_shape=(S((8, 4096, 128), BF), S((128, 4096), BF), S((8, 64, 128), BF), S((128, 1024), BF)),
        in_specs=[any_] * 9,
        out_specs=[any_, vmem, vmem, vmem],
        scratch_shapes=[
            V((16384, TT), BF),
            V((16384, 128), BF),
            V((2048, 1024), BF),
            V((2, 4, 4, 512, 128), BF),
            V((2, 2, 4, 256, 128), BF),
            V((2, 2, 4, 512, 128), BF),
            V((2, 2, 256, 128), BF),
            V((2, 2, 512, 128), BF),
            V((2, 4, 128, 512), BF),
            V((2, 4, 128, 128), BF),
            V((128, TT), BF), V((TT, 128), BF), V((128, TT), BF), V((TT, 128), BF),
            V((80, TT), F32), V((1, TT), F32), V((16, 1, TT), F32), V((64, TT), F32),
            V((128, T), BF),
            V((8, 128, 128), BF), V((8, 128, 128), BF), V((1024, 128), BF), V((T, 128), BF),
            V((64, 4096), BF), V((128, 4096), BF),
            V((1, 4096), F32), V((1, 4096), F32),
            D((256,)), D((32,)), D((4, 2, 2)), D((4, 2, 2)), D((4, 2, 2)), D((8,)), D((2, 4, 4, 2)),
            D((2, 2, 4)), D((2, 2, 4)), D((2, 2)), D((2, 2)), D((4, 2, 4)), D((8,)), D((8,)),
        ],
        compiler_params=pltpu.CompilerParams(
            collective_id=0, has_side_effects=True, vmem_limit_bytes=67043328
        ),
    )(target, source, gain_t.reshape(1, -1), gain_s.reshape(1, -1), wq, wk, wv, wo, go)


def norm_back(matrix, scaling, upstream):
    widened = matrix.astype(F32)
    factor = lax.rsqrt(jnp.mean(widened * widened, axis=-1, keepdims=True) + EPS)
    weighted = upstream * scaling
    inner = jnp.mean(widened * weighted, axis=-1, keepdims=True)
    return factor * weighted - widened * factor * factor * factor * inner


def shards(target, source, gain_t, gain_s, wq, wk, wv, wo, go):
    wq_all, gop, dq, dkv = mega(target, source, gain_t, gain_s, wq, wk, wv, wo, go)
    grad_xn = lax.dot_general(dq, wq_all, (((0, 2), (0, 2)), ((), ())), preferred_element_type=F32)
    grad_target = norm_back(target, gain_t, grad_xn)
    grad_sn = dot_t(dkv[:, :512], wk) + dot_t(dkv[:, 512:], wv)
    grad_source = norm_back(source, gain_s, grad_sn)
    return grad_target, grad_source, gop.astype(F32)


def solution(mesh):
    rows = P(("sp", "tp"), None)
    return jax.shard_map(
        shards,
        mesh=mesh,
        in_specs=(rows, rows, P(), P(), P(None, "tp"), P(), P(), P("tp", None), rows),
        out_specs=(rows, rows, P("tp", None)),
        check_vma=False,
    )
```

time: 476 us -> 169 us (0.36)
  waiting for transfers between devices: 170 us -> 0 us
  Pallas kernels: 0 us -> 152 us
  local copies, waits for them, and re-layouts: 113 us -> 1.94 us
  matrix products: 112 us -> 9.36 us
  other arithmetic: 31.2 us -> 4.7 us
  between operations: 14 us -> 0.7 us
  blocking collectives: 12.3 us -> 0 us
  loops' own time: 12 us -> 0 us
  starting transfers between devices: 7.12 us -> 0 us
    pallas_call x0 -> x1, Pallas kernels: none -> 152 us  [mega(): pl.pallas_call(kernel, out_shape=(S((8, 4096, 128), BF), S((128, 4096), B...]
    dot_general x118 -> x3, matrix products: 112 us -> 9.36 us  [the longest x1 6.26 us: shards(): lax.dot_general(dq, wq_all, (((0, 2), (0, 2)), ((), ())), preferred_eleme...]
    reduce_scatter x2 -> x0, waiting for transfers between devices: 102 us -> none  [the longest x1 70.6 us: shards(): lax.psum_scatter(pair_store.astype(jnp.bfloat16), 'sp', scatter_dimension...]
    all_gather x2 -> x0, waiting for transfers between devices: 67.6 us -> none  [the longest x1 50.4 us: shards(): lax.all_gather(own_pairs, 'sp', axis=0, tiled=True)]
    squeeze x32 -> x0, local copies, waits for them, and re-layouts: 31.2 us -> none  [shards(): lax.scan(absorb_advance, (start_max, start_sum, start_acc), blocks)]
    unnamed x17 -> x14, local copies, waits for them, and re-layouts: 33.1 us -> 1.94 us
    reshape x1 -> x0, local copies, waits for them, and re-layouts: 14.7 us -> none  [split_arrived(): arrived.reshape(row_count // block_size, block_size, key_count, 2, HD)]
    dynamic_update_slice x32 -> x0, local copies, waits for them, and re-layouts: 14.4 us -> none  [collect_advance(): lax.dynamic_update_slice_in_dim(pair_store, stacked, where_rows, 0)]
  transfers between devices with their start and end apart: 6 -> 0, of which waited for: 4 -> 0; matrix products, arithmetic and copies ran while one was open for 31% -> 0% of each run, Pallas kernels for 0% -> 0%
where the time goes in v1:
time: 169 us; the launch traced here: 168 us
  Pallas kernels  152 us (90%)
  matrix products  9.36 us (6%)
  other arithmetic  4.7 us (3%)
  local copies, waits for them, and re-layouts  1.94 us (1%)
    pallas_call x1, Pallas kernels, mega(): pl.pallas_call(kernel, out_shape=(S((8, 4096, 128), BF), S((128, 4096), B...  152 us
    dot_general x1, matrix products, shards(): lax.dot_general(dq, wq_all, (((0, 2), (0, 2)), ((), ())), preferred_eleme...  6.26 us

profile of v1, /device:TPU:1, one launch (start us, length us, event | category | flops | bytes accessed | tf_op | source)
XLA Modules:
  0.0 168.4 jit_solution(17129897470301794182)
XLA Ops:
  0.6 151.7 %shard_map.112 = (bf16[8,4096,128]{2,1,0:T(8,128)(2,1)}, bf16[128,4096]{1,0:T(8,128)(2,1)}, bf16[8,64,128]{2,1,0:T(8,128)(2,1)}, bf16[128,1024]{1,0:T(8,128)(2,1)}) custom-call(bf16[64,4096]{1,0:T(8,128)(2,1)} %tgt.1, bf16[128,4096]{1,0:T(8,128)(2,1)} %src.1, f32[1,4096]{1,0:T(1,128)} %bitcast.10, f32[1,4096]{1,0:T(1,128)} %bitcast.11, ...), custom_call_target="tpu_custom_call" | custom-call | tf_op jit(solution)/shard_map/pallas_call | solution.py:541
  152.4 0.0 copy-start.3
  152.4 6.3 %fusion.8 = (f32[64]{0:T(128)S(1)}, f32[64]{0:T(128)S(1)}, f32[64,4096]{1,0:T(8,128)S(1)}) fusion(bf16[64,4096]{1,0:T(8,128)(2,1)} %tgt.1, f32[4096]{0:T(1024)} %param.11, bf16[8,64,128]{2,1,0:T(8,128)(2,1)} %get-tuple-element.7, bf16[8,4096,128]{2,1,0:T(8,128)(2,1)} %get-tuple-element.8), kind=kOutput, calls=%fused_computation.16 | convolution fusion | flops 538443648 | bytes 10109440 | tf_op jit(solution)/shard_map/dot_general | solution.py:582
  158.6 0.0 copy-start.4
  158.7 0.0 copy-done.3
  158.7 0.0 copy-start.1
  158.7 1.3 fusion.12
  160.0 0.0 copy-done.4
  160.0 0.0 copy-start.5
  160.0 1.5 convert_element_type.11
  161.5 0.8 copy-done.1
  162.3 0.1 copy-done.5
  162.4 0.0 copy-start
  162.4 0.0 copy-start.2
  162.4 0.0 copy-start.6
  162.4 1.5 fusion.15
  163.9 0.7 copy-done
  164.6 0.3 copy-done.2
  164.9 0.0 copy-done.6
  164.9 1.6 fusion.2
  166.5 1.9 %fusion.6 = f32[128,4096]{1,0:T(8,128)} fusion(bf16[128,4096]{1,0:T(8,128)(2,1)S(1)} %copy-done.2, f32[128,4096]{1,0:T(8,128)S(1)} %get-tuple-element.16, f32[128]{0:T(128)S(1)} %get-tuple-element.20, f32[128]{0:T(128)S(1)} %get-tuple-element.19), kind=kLoop, calls=%fused_computation.11 | loop fusion | flops 3670016 | bytes 5243904 | tf_op jit(solution)/shard_map/sub | solution.py:577
  (2 shorter events, 0.0 us)
Async XLA Ops:
  152.4 6.3 %copy-start.3 = (bf16[64,4096]{1,0:T(8,128)(2,1)S(1)}, bf16[64,4096]{1,0:T(8,128)(2,1)}, u32[]{:S(2)}) copy-start(bf16[64,4096]{1,0:T(8,128)(2,1)} %tgt.1) | copy-start | bytes 1572868
  158.6 1.3 copy-start.4
  158.7 3.6 %copy-start.1 = (bf16[4096,512]{1,0:T(8,128)(2,1)S(1)}, bf16[4096,512]{1,0:T(8,128)(2,1)}, u32[]{:S(2)}) copy-start(bf16[4096,512]{1,0:T(8,128)(2,1)} %wk.1) | copy-start | bytes 12582916
  160.0 2.5 %copy-start.5 = (bf16[128,1024]{1,0:T(8,128)(2,1)S(1)}, bf16[128,1024]{1,0:T(8,128)(2,1)}, u32[]{:S(2)}) copy-start(bf16[128,1024]{1,0:T(8,128)(2,1)} %get-tuple-element.9) | copy-start | bytes 786436
  162.4 2.2 %copy-start = (bf16[4096,512]{1,0:T(8,128)(2,1)S(1)}, bf16[4096,512]{1,0:T(8,128)(2,1)}, u32[]{:S(2)}) copy-start(bf16[4096,512]{1,0:T(8,128)(2,1)} %wv.1) | copy-start | bytes 12582916
  162.4 2.5 %copy-start.2 = (bf16[128,4096]{1,0:T(8,128)(2,1)S(1)}, bf16[128,4096]{1,0:T(8,128)(2,1)}, u32[]{:S(2)}) copy-start(bf16[128,4096]{1,0:T(8,128)(2,1)} %src.1) | copy-start | bytes 3145732
  162.4 2.5 %copy-start.6 = (f32[4096]{0:T(1024)S(1)}, f32[4096]{0:T(1024)}, u32[]{:S(2)}) copy-start(f32[4096]{0:T(1024)} %param.12) | copy-start | bytes 49156

commit v2 on v1

--- a/solution.py
+++ b/solution.py
@@ -15,6 +15,7 @@
 T = 512
 TT = 2 * T
 U = 1024
+TG0 = 6144
 XN0 = 4096
 
 
@@ -93,9 +94,15 @@
             return self.net.push(src, src, self.recv.at[d, 1, h], tp=at.ring(0, 1))
         return self.net.push(src, src, self.recv.at[(d - way) % 4, 0, h], tp=at.ring(way, 0))
 
+    def begin_first(self):
+        return [self.send(0, 0, 1), self.send(0, 1, -1)]
+
+    def begin_rest(self):
+        s = self.send
+        return [s(0, 1, 1), s(0, 0, -1), s(0, 0, 0), s(0, 1, 0)]
+
     def begin(self):
-        s = self.send
-        return [s(0, 0, 1), s(0, 1, -1), s(0, 1, 1), s(0, 0, -1), s(0, 0, 0), s(0, 1, 0)]
+        return self.begin_first() + self.begin_rest()
 
     def come(self, d, h, sib):
         at = self.net.at
@@ -137,6 +144,10 @@
         for piece, way in ((0, 1), (1, -1), (1, 1), (0, -1)):
             for half in (0, 1):
                 sent.append(self.send(half, 0, 0, piece, 0, way))
+        return sent
+
+    def begin_second(self):
+        sent = []
         for piece, way in ((0, 1), (1, -1), (1, 1), (0, -1)):
             for half in (0, 1):
                 sent.append(self.send(half, 0, 0, piece, 1, way))
@@ -173,14 +184,16 @@
 
 def kernel(
     tgt, src, gain_t, gain_s, wq, wk, wv, wo, go,
-    wq_all, gop, dq_loc, dkv_loc,
+    wq_all, gop, grad_t, grad_s,
     E, kv, gg, dkv, hop, end1, hop2, end2, ar1, ar2,
-    qT, qP, dT, dP, acc, m_run, m_unit, dqT, oT, pr, back, fin, dqs,
-    tgt_v, wo_v, gt_v, gs_v,
+    qT, qP, dT, dP, acc, m_run, m_unit, s0, s1, top0, top1, oT, back, dq_loc,
+    wo_v, gt_v, gs_v,
     send_sems, load_sems, r_xn, r_gg, r_wq, r_a2a, r_kv, r_rs1, r_rs2, r_rs3, r_rs4, r_ar, r_dq, r_dkv,
 ):
     src_v = gop
     arP = wo_v
+    dqT = acc.at[pl.ds(0, 64), :]
+    fin, dqs = qP, dP
     at = Coords()
     net = Net(at, send_sems, E)
     lane = lax.broadcasted_iota(jnp.int32, (1, 128), 1)
@@ -202,7 +215,6 @@
         for k in range(4)
     ]
     loads = [
-        pltpu.make_async_copy(tgt, tgt_v, load_sems.at[0]),
         pltpu.make_async_copy(gain_t, gt_v, load_sems.at[1]),
         pltpu.make_async_copy(src, src_v, load_sems.at[2]),
         pltpu.make_async_copy(gain_s, gs_v, load_sems.at[3]),
@@ -210,13 +222,19 @@
         pltpu.make_async_copy(wv, E.at[pl.ds(0, 4096), pl.ds(512, 512)], load_sems.at[5]),
         pltpu.make_async_copy(wo, wo_v, load_sems.at[6]),
     ]
+    loads_t = [
+        pltpu.make_async_copy(
+            tgt.at[:, pl.ds(1024 * k, 1024)], E.at[pl.ds(TG0 + 64 * k, 64), :], load_sems.at[12 + k]
+        )
+        for k in range(4)
+    ]
     loads_w = [
         pltpu.make_async_copy(
             wq.at[pl.ds(512 * k, 512), :], dkv.at[0, k // 4, k % 4], load_sems.at[16 + k]
         )
         for k in range(8)
     ]
-    for load in loads + loads_w + gg_own:
+    for load in loads_t + loads + loads_w + gg_own:
         load.start()
 
     def xn_place(j, h):
@@ -232,31 +250,36 @@
     rows_g = RowsGather(net, gg_place, r_gg)
     rows_w = RowsGather(net, wq_place, r_wq)
 
+    for load in loads_t:
+        load.wait()
     loads[0].wait()
-    loads[1].wait()
-    xn = normalize(tgt_v[...], gt_v[...])
+    xn = normalize(jnp.concatenate([E[TG0 + 64 * k : TG0 + 64 * k + 64, :] for k in range(4)], axis=1), gt_v[...])
     for k in range(4):
         E[pl.ds(pl.multiple_of(XN0 + at.tp * 256 + 64 * k, 64), 64), :] = xn[:, 1024 * k : 1024 * k + 1024]
     pl.semaphore_wait(barrier, len(others))
-    sent_x = rows_x.begin()
-
+    sent_x = rows_x.begin_first()
+
+    loads[1].wait()
     loads[2].wait()
+    sn = normalize(src_v[...], gs_v[...])
     loads[3].wait()
-    sn = normalize(src_v[...], gs_v[...])
     loads[4].wait()
-    loads[5].wait()
     pairs = dot(sn, E[0:4096, :])
     for g in range(4):
         kb = pairs[:, 128 * g : 128 * g + 128]
         vb = pairs[:, 512 + 128 * g : 512 + 128 * g + 128]
-        pr[2 * g] = jnp.where(low, kb, pltpu.roll(vb, 64, 1)).astype(BF)
-        pr[2 * g + 1] = jnp.where(low, pltpu.roll(kb, 64, 1), vb).astype(BF)
+        dP[256 * g : 256 * g + 128, :] = jnp.where(low, kb, pltpu.roll(vb, 64, 1)).astype(BF)
+        dP[256 * g + 128 : 256 * g + 256, :] = jnp.where(low, pltpu.roll(kb, 64, 1), vb).astype(BF)
     mine = kv.at[pl.ds(pl.multiple_of(at.sp * 1024 + at.tp * 128, 128), 128), :]
-    sent = []
+    sent, sent_a2a = [], []
     for j in (4, 3, 5, 2, 6, 1, 7):
         to = (at.tp + j) % 8
-        sent.append(net.push(pr.at[to], mine, r_a2a.at[8 - j], tp=to))
-    mine[...] = pr[at.tp]
+        place = dP.at[pl.ds(pl.multiple_of(to * 128, 128), 128), :]
+        sent_a2a.append(net.push(place, mine, r_a2a.at[8 - j], tp=to))
+    mine[...] = dP[pl.ds(pl.multiple_of(at.tp * 128, 128), 128), :]
+    for d, h in FIRST:
+        sent_x += rows_x.come(d, h, 0)
+    sent_x += rows_x.begin_rest()
     for j in range(1, 8):
         frm = (at.tp + j) % 8
         net.arrive(kv.at[pl.ds(pl.multiple_of(at.sp * 1024 + frm * 128, 128), 128), :], r_a2a.at[j])
@@ -264,7 +287,7 @@
     sent += pairs_g.begin()
     for load in gg_own:
         load.wait()
-    loads[6].wait()
+    loads[5].wait()
     for load in loads_w:
         load.wait()
     own_w = [
@@ -276,14 +299,18 @@
     for copy in own_w:
         copy.start()
 
-    for d, h in FIRST:
+    for e in PHASE1[:2]:
+        sent += pairs_g.come(*e)
+    sent += pairs_g.begin_second()
+    for e in PHASE1[2:4]:
+        sent += pairs_g.come(*e)
+    for d, h in SECOND[:2]:
         sent_x += rows_x.come(d, h, 0)
-    sent += rows_g.begin()
-    for e in PHASE1:
+    for e in PHASE1[4:] + PHASE2[:2]:
         sent += pairs_g.come(*e)
-    for d, h in SECOND:
+    for d, h in SECOND[2:]:
         sent_x += rows_x.come(d, h, 0)
-    for e in PHASE2:
+    for e in PHASE2[2:4]:
         sent += pairs_g.come(*e)
     for d, h in SIBS:
         rows_x.come(d, h, 1)
@@ -300,15 +327,78 @@
     for k in range(1, 4):
         q += dot(gathered(E, XN0, k), wq_rows(k))
     q = q.astype(BF).astype(F32)
-    net.sent(sent_x)
-
-    for d, h in FIRST:
-        sent += rows_g.come(d, h, 0)
-    for copy in own_w:
-        copy.wait()
-    sent += rows_w.begin()
-    for d, h in SECOND:
-        sent += rows_g.come(d, h, 0)
+    net.sent(sent_x + sent_a2a)
+
+    for h, a in enumerate((jnp.where(low, q, 0.0), jnp.where(low, pltpu.roll(q, 64, 1), 0.0))):
+        r = slice(h * T, h * T + T)
+        qP[r, :] = a.astype(BF)
+        qT[:, r] = (a * 0.125).T.astype(BF)
+
+    acc[...] = jnp.zeros_like(acc)
+    m_run[...] = jnp.full_like(m_run, -jnp.inf)
+    ones = jnp.ones((16, 512), BF)
+    work, tops = (s0, s1), (top0, top1)
+
+    def kv_rows(half, a, b):
+        start = pl.multiple_of(at.block(half, a, b) * 1024 + half * 512, 512)
+        return kv[pl.ds(start, 512), :]
+
+    def weights_at(half, u):
+        return pl.ds(pl.multiple_of(u * U + half * 512, 512), 512)
+
+    def scores(half, u):
+        s = dot(kv_rows(half, order(u % 4), order(u // 4)), qT[...])
+        work[half][...] = s
+        tops[half][...] = jnp.max(s, axis=0, keepdims=True)
+
+    def absorb(half, u):
+        m_old = m_run[...]
+        m_new = jnp.maximum(m_old, tops[half][...])
+        shrink = jnp.exp(m_old - m_new)
+        e = jnp.exp(work[half][...] - m_new).astype(BF)
+        E[weights_at(half, u), :] = e
+        m_run[...] = m_new
+        m_unit[pl.ds(2 * u + half, 1)] = m_new[None]
+        block = kv_rows(half, order(u % 4), order(u // 4))
+        vt = block.astype(F32).T.astype(BF)[64:128, :]
+        acc[...] = acc[...] * shrink + dot(jnp.concatenate([vt, ones], axis=0), e)
+
+    def begin_w():
+        for copy in own_w:
+            copy.wait()
+        sent.extend(rows_w.begin())
+
+    def gg_come(places):
+        for d, h in places:
+            sent.extend(rows_g.come(d, h, 0))
+
+    def pairs_come(places):
+        for e in places:
+            sent.extend(pairs_g.come(*e))
+
+    heads = {
+        0: lambda: (sent.extend(rows_g.begin()), pairs_come(PHASE2[4:8])),
+        1: lambda: pairs_come(PHASE2[8:12]),
+        2: lambda: pairs_come(PHASE2[12:15]),
+        3: lambda: pairs_come(PHASE2[15:18]),
+        5: lambda: pairs_come(PHASE2[18:20]),
+        6: lambda: (gg_come(FIRST), pairs_come(PHASE2[20:22])),
+        8: lambda: pairs_come(PHASE2[22:24]),
+        10: lambda: gg_come(SECOND[:2]),
+        14: lambda: (gg_come(SECOND[2:]), begin_w()),
+    }
+
+    def fwd(u, _):
+        for k, f in heads.items():
+            pl.when(u == k)(lambda f=f: f() and None)
+        scores(1, u)
+        absorb(0, u)
+        scores(0, (u + 1) % 16)
+        absorb(1, u)
+        return 0
+
+    scores(0, 0)
+    lax.fori_loop(0, 16, fwd, 0)
     for d, h in SIBS:
         rows_g.come(d, h, 1)
     do = dot_t(gathered(gg, 0, 0), wo_v[:, 0:1024])
@@ -316,50 +406,18 @@
         do += dot_t(gathered(gg, 0, k), wo_v[:, 1024 * k : 1024 * k + 1024])
     do = do.astype(BF).astype(F32)
 
-    q0 = jnp.where(low, q, 0.0)
-    q1 = jnp.where(low, pltpu.roll(q, 64, 1), 0.0)
-    d0 = jnp.where(low, 0.0, pltpu.roll(do, 64, 1))
-    d1 = jnp.where(low, 0.0, do)
-    for h, (a, b) in enumerate(((q0, d0), (q1, d1))):
+    for h, b in enumerate((jnp.where(low, 0.0, pltpu.roll(do, 64, 1)), jnp.where(low, 0.0, do))):
         r = slice(h * T, h * T + T)
-        qP[r, :] = a.astype(BF)
         dP[r, :] = b.astype(BF)
-        qT[:, r] = (a * 0.125).T.astype(BF)
         dT[:, r] = (b * 0.125).T.astype(BF)
 
-    acc[...] = jnp.zeros_like(acc)
-    m_run[...] = jnp.full_like(m_run, -jnp.inf)
-    dqT[...] = jnp.zeros_like(dqT)
-    ones = jnp.ones((16, U), BF)
-
-    def unit_kv(a, b):
-        parts = []
-        for half in (0, 1):
-            start = pl.multiple_of(at.block(half, a, b) * 1024 + half * 512, 512)
-            parts.append(kv[pl.ds(start, 512), :])
-        return jnp.concatenate(parts, axis=0)
-
-    def fwd(u, _):
-        block = unit_kv(order(u % 4), order(u // 4))
-        s = dot(block, qT[...])
-        m_old = m_run[...]
-        m_new = jnp.maximum(m_old, jnp.max(s, axis=0, keepdims=True))
-        shrink = jnp.exp(m_old - m_new)
-        e = jnp.exp(s - m_new).astype(BF)
-        E[pl.ds(pl.multiple_of(u * U, U), U), :] = e
-        m_run[...] = m_new
-        m_unit[pl.ds(u, 1)] = m_new[None]
-        vt = block.astype(F32).T.astype(BF)[64:128, :]
-        acc[...] = acc[...] * shrink + dot(jnp.concatenate([vt, ones], axis=0), e)
-        return 0
-
-    lax.fori_loop(0, 16, fwd, 0)
     inv = 1.0 / acc[64:65, :]
     o = (acc[0:64, :] * inv).astype(BF)
     oT[0:64, :] = o[:, 0:T]
     oT[64:128, :] = o[:, T:]
     delta = jnp.sum(dT[64:128, :].astype(F32) * o.astype(F32), axis=0, keepdims=True)
     m_end = m_run[...]
+    dqT[...] = jnp.zeros((64, TT), F32)
 
     for k in range(4):
         arP[:, 1024 * k : 1024 * k + 1024] = dot(oT[...], gathered(gg, 0, k)).astype(BF)
@@ -375,24 +433,24 @@
     def ar_1():
         for half in (0, 1):
             for a in (1, 3, 2):
-                sent.append(net.push(arP.at[:, wide_col(half, a)], ar1.at[half, 4 - a], r_ar.at[0, half, 4 - a], sp=at.block(half, a, 0)))
+                sent.append(net.push(arP.at[:, wide_col(half, a)], ar1.at[half, 3 - a], r_ar.at[0, half, 4 - a], sp=at.block(half, a, 0)))
 
     def ar_2():
         for half in (0, 1):
             total = arP[:, wide_col(half, 0)].astype(F32)
             for a in (1, 2, 3):
-                net.arrive(ar1.at[half, a], r_ar.at[0, half, a])
-                total += ar1[half, a].astype(F32)
+                net.arrive(ar1.at[half, a - 1], r_ar.at[0, half, a])
+                total += ar1[half, a - 1].astype(F32)
             arP[:, wide_col(half, 0)] = total.astype(BF)
             for b in (1, 3, 2):
-                sent.append(net.push(arP.at[:, slim_col(half, b)], ar2.at[half, 4 - b], r_ar.at[1, half, 4 - b], sp=at.block(half, 0, b)))
+                sent.append(net.push(arP.at[:, slim_col(half, b)], ar2.at[half, 3 - b], r_ar.at[1, half, 4 - b], sp=at.block(half, 0, b)))
 
     def ar_3():
         for half in (0, 1):
             total = arP[:, slim_col(half, 0)].astype(F32)
             for b in (1, 2, 3):
-                net.arrive(ar2.at[half, b], r_ar.at[1, half, b])
-                total += ar2[half, b].astype(F32)
+                net.arrive(ar2.at[half, b - 1], r_ar.at[1, half, b])
+                total += ar2[half, b - 1].astype(F32)
             gop[:, slim_col(half, 0)] = total.astype(BF)
             for b in (1, 3, 2):
                 place = gop.at[:, slim_col(half, 0)]
@@ -414,8 +472,15 @@
     def add_to(place, arrived):
         place[...] = (place[...].astype(F32) + arrived[...].astype(F32)).astype(BF)
 
+    def back_place(i):
+        group = i // 4
+        mid = (group + 1) // 2 % 2
+        ia = mid * (2 - i % 2) + (1 - mid) * (3 - group)
+        ib = mid * (3 - (i + 4) // 2 + 4) + (1 - mid) * (3 - i % 4)
+        return order(ia), order(ib), ib * 4 + ia
+
     def after(i):
-        a, b = [2, 3, 1, 0][i // 4], [2, 3, 1, 0][i % 4]
+        a, b, _ = back_place(i)
         for half in (0, 1):
             piece = dkv.at[half, a, b]
             top, bottom = piece.at[pl.ds(0, 256), :], piece.at[pl.ds(256, 256), :]
@@ -457,6 +522,59 @@
                         total += end2[half, side].astype(F32)
                     fin[half * 512 : half * 512 + 512, :] = total.astype(BF)
 
+    def projected(half, i):
+        a, b, _ = back_place(i)
+        work[half][...] = dot(kv_rows(half, a, b), dT[...])
+
+    def gradients(half, i):
+        a, b, u = back_place(i)
+        scale = jnp.exp(m_unit[2 * u + half] - m_end) * inv
+        p = E[weights_at(half, u), :].astype(F32) * scale
+        g = (p * (work[half][...] - delta)).astype(BF)
+        dkv[half, a, b] = (dot(g, qP[...]) + dot(p.astype(BF), dP[...])).astype(BF)
+        kt = kv_rows(half, a, b).astype(F32).T.astype(BF)[0:64, :]
+        dqT[...] += dot(kt, g)
+
+    def spare(i, c):
+        return back_place(i)[2] * U + c
+
+    def loads_last(k):
+        if 2 <= k < 6:
+            c = k - 2
+            return [
+                pltpu.make_async_copy(
+                    w.at[pl.ds(1024 * c, 1024), :],
+                    E.at[pl.ds(spare(c, 0), 1024), pl.ds(512 * n, 512)],
+                    load_sems.at[8 * n + c],
+                )
+                for n, w in enumerate((wk, wv))
+            ]
+        if k == 6:
+            return [
+                pltpu.make_async_copy(
+                    rows.at[:, pl.ds(1024 * c, 1024)],
+                    E.at[pl.ds(spare(4, first + count * c), count), :],
+                    load_sems.at[16 + c + n],
+                )
+                for rows, first, count, n in ((src, 0, 128, 0), (tgt, 512, 64, 4))
+                for c in range(4)
+            ]
+        if k in (14, 15):
+            return [
+                pltpu.make_async_copy(
+                    wq_all.at[j, pl.ds(1024 * c, 1024), :],
+                    E.at[pl.ds(spare(5 + c, 0), 1024), pl.ds(128 * j, 128)],
+                    load_sems.at[32 + 8 * c + j],
+                )
+                for c in ((0, 1) if k == 14 else (2, 3))
+                for j in range(8)
+            ]
+        return []
+
+    def load_ahead(k):
+        for copy in loads_last(k):
+            copy.start()
+
     def bwd(i, _):
         for k in range(16):
             if k == 3:
@@ -470,39 +588,37 @@
 
             @pl.when(i == k)
             def _(k=k, extra=extra):
+                load_ahead(k)
                 for f in extra:
                     f()
                 if k > 0:
                     after(k - 1)
-                if k == 2:
+                if k == 3:
                     for d, h in FIRST:
                         sent.extend(rows_w.come(d, h, 0))
-                if k == 9:
-                    for d, h in SECOND:
+                if k == 6:
+                    for d, h in SECOND[:2]:
                         sent.extend(rows_w.come(d, h, 0))
-
-        ia, ib = 3 - i // 4, 3 - i % 4
-        a, b = order(ia), order(ib)
-        block = unit_kv(a, b)
-        dp = dot(block, dT[...])
-        u = ib * 4 + ia
-        scale = jnp.exp(m_unit[u] - m_end) * inv
-        p = E[pl.ds(pl.multiple_of(u * U, U), U), :].astype(F32) * scale
-        g = (p * (dp - delta)).astype(BF)
-        both = dot(g, qP[...]) + dot(p.astype(BF), dP[...])
-        both = both.astype(BF)
-        dkv[0, a, b] = both[0:512, :]
-        dkv[1, a, b] = both[512:1024, :]
-        kt = block.astype(F32).T.astype(BF)[0:64, :]
-        dqT[...] += dot(kt, g)
+                if k == 11:
+                    for d, h in SECOND[2:]:
+                        sent.extend(rows_w.come(d, h, 0))
+                if k == 13:
+                    for d, h in SIBS:
+                        rows_w.come(d, h, 1)
+
+        projected(1, i)
+        gradients(0, i)
+        projected(0, (i + 1) % 16)
+        gradients(1, i)
         return 0
 
     ar_1()
+    projected(0, 0)
     lax.fori_loop(0, 16, bwd, 0)
 
     grad = dqT[...]
     grad = jnp.concatenate([grad[:, 0:T], grad[:, T:]], axis=0).T.astype(BF)
-    dqs[...] = grad
+    dqs[0:T, :] = grad
     for j in (4, 3, 5, 2, 6, 1, 7):
         to = (at.tp + j) % 8
         sent.append(net.push(
@@ -518,19 +634,55 @@
             back.at[at.tp], r_dkv.at[8 - j], tp=to,
         ))
     back[at.tp] = fin[pl.ds(pl.multiple_of(at.tp * 128, 128), 128), :]
-    ar_5()
-    for d, h in SIBS:
-        rows_w.come(d, h, 1)
     for j in range(1, 8):
         frm = (at.tp + j) % 8
         net.arrive(dq_loc.at[frm], r_dq.at[j])
+    for k in range(16):
+        for copy in loads_last(k):
+            copy.wait()
+
+    def finish(rows, x_of, gain, up_of, buf, out, sems):
+        squares = jnp.zeros((rows, 1), F32)
+        inner = jnp.zeros((rows, 1), F32)
+        for c in range(4):
+            x = x_of(c).astype(F32)
+            weighted = up_of(c) * gain[:, 1024 * c : 1024 * c + 1024]
+            buf[rows * c : rows * c + rows, :] = weighted
+            squares += jnp.sum(x * x, axis=-1, keepdims=True)
+            inner += jnp.sum(x * weighted, axis=-1, keepdims=True)
+        factor = lax.rsqrt(squares / 4096 + EPS)
+        pull = factor * factor * factor * (inner / 4096)
+        copies = []
+        for c in range(4):
+            r = slice(rows * c, rows * c + rows)
+            buf[r, :] = factor * buf[r, :] - x_of(c).astype(F32) * pull
+            copies.append(pltpu.make_async_copy(
+                buf.at[pl.ds(rows * c, rows), :], out.at[:, pl.ds(1024 * c, 1024)], load_sems.at[sems + c]
+            ))
+            copies[-1].start()
+        return copies
+
+    dq_rows = jnp.concatenate([dq_loc[j] for j in range(8)], axis=1)
+    outs = finish(
+        64, lambda c: E[pl.ds(spare(4, 512 + 64 * c), 64), :], gt_v,
+        lambda c: dot_t(dq_rows, E[pl.ds(spare(5 + c, 0), 1024), :]), s1, grad_t, 64,
+    )
     for j in range(1, 8):
         frm = (at.tp + j) % 8
         net.arrive(back.at[frm], r_dkv.at[j])
+    keys, values = [], []
     for g in range(4):
         even, odd = back[2 * g].astype(F32), back[2 * g + 1].astype(F32)
-        dkv_loc[:, 128 * g : 128 * g + 128] = jnp.where(low, even, pltpu.roll(odd, 64, 1)).astype(BF)
-        dkv_loc[:, 512 + 128 * g : 640 + 128 * g] = jnp.where(low, pltpu.roll(even, 64, 1), odd).astype(BF)
+        keys.append(jnp.where(low, even, pltpu.roll(odd, 64, 1)).astype(BF))
+        values.append(jnp.where(low, pltpu.roll(even, 64, 1), odd).astype(BF))
+    dkv_rows = jnp.concatenate(keys + values, axis=1)
+    outs += finish(
+        128, lambda c: E[pl.ds(spare(4, 128 * c), 128), :], gs_v,
+        lambda c: dot_t(dkv_rows, E[pl.ds(spare(c, 0), 1024), :]), s0, grad_s, 68,
+    )
+    ar_5()
+    for copy in outs:
+        copy.wait()
     net.sent(sent)
 
 
@@ -540,9 +692,9 @@
     V, D, S = pltpu.VMEM, pltpu.SemaphoreType.DMA, jax.ShapeDtypeStruct
     return pl.pallas_call(
         kernel,
-        out_shape=(S((8, 4096, 128), BF), S((128, 4096), BF), S((8, 64, 128), BF), S((128, 1024), BF)),
+        out_shape=(S((8, 4096, 128), BF), S((128, 4096), BF), S((64, 4096), F32), S((128, 4096), F32)),
         in_specs=[any_] * 9,
-        out_specs=[any_, vmem, vmem, vmem],
+        out_specs=[any_, vmem, any_, any_],
         scratch_shapes=[
             V((16384, TT), BF),
             V((16384, 128), BF),
@@ -552,15 +704,16 @@
             V((2, 2, 4, 512, 128), BF),
             V((2, 2, 256, 128), BF),
             V((2, 2, 512, 128), BF),
-            V((2, 4, 128, 512), BF),
-            V((2, 4, 128, 128), BF),
+            V((2, 3, 128, 512), BF),
+            V((2, 3, 128, 128), BF),
             V((128, TT), BF), V((TT, 128), BF), V((128, TT), BF), V((TT, 128), BF),
-            V((80, TT), F32), V((1, TT), F32), V((16, 1, TT), F32), V((64, TT), F32),
+            V((80, TT), F32), V((1, TT), F32), V((32, 1, TT), F32),
+            V((512, TT), F32), V((512, TT), F32), V((1, TT), F32), V((1, TT), F32),
             V((128, T), BF),
-            V((8, 128, 128), BF), V((8, 128, 128), BF), V((1024, 128), BF), V((T, 128), BF),
-            V((64, 4096), BF), V((128, 4096), BF),
+            V((8, 128, 128), BF), V((8, 64, 128), BF),
+            V((128, 4096), BF),
             V((1, 4096), F32), V((1, 4096), F32),
-            D((256,)), D((32,)), D((4, 2, 2)), D((4, 2, 2)), D((4, 2, 2)), D((8,)), D((2, 4, 4, 2)),
+            D((256,)), D((80,)), D((4, 2, 2)), D((4, 2, 2)), D((4, 2, 2)), D((8,)), D((2, 4, 4, 2)),
             D((2, 2, 4)), D((2, 2, 4)), D((2, 2)), D((2, 2)), D((4, 2, 4)), D((8,)), D((8,)),
         ],
         compiler_params=pltpu.CompilerParams(
@@ -569,21 +722,9 @@
     )(target, source, gain_t.reshape(1, -1), gain_s.reshape(1, -1), wq, wk, wv, wo, go)
 
 
-def norm_back(matrix, scaling, upstream):
-    widened = matrix.astype(F32)
-    factor = lax.rsqrt(jnp.mean(widened * widened, axis=-1, keepdims=True) + EPS)
-    weighted = upstream * scaling
-    inner = jnp.mean(widened * weighted, axis=-1, keepdims=True)
-    return factor * weighted - widened * factor * factor * factor * inner
-
-
-def shards(target, source, gain_t, gain_s, wq, wk, wv, wo, go):
-    wq_all, gop, dq, dkv = mega(target, source, gain_t, gain_s, wq, wk, wv, wo, go)
-    grad_xn = lax.dot_general(dq, wq_all, (((0, 2), (0, 2)), ((), ())), preferred_element_type=F32)
-    grad_target = norm_back(target, gain_t, grad_xn)
-    grad_sn = dot_t(dkv[:, :512], wk) + dot_t(dkv[:, 512:], wv)
-    grad_source = norm_back(source, gain_s, grad_sn)
-    return grad_target, grad_source, gop.astype(F32)
+def shards(*args):
+    _, grad_out_proj, grad_target, grad_source = mega(*args)
+    return grad_target, grad_source, grad_out_proj.astype(F32)
 
 
 def solution(mesh):

time: 169 us -> 133 us (0.79)
  Pallas kernels: 152 us -> 126 us
  matrix products: 9.36 us -> 0 us
  other arithmetic: 4.7 us -> 2.91 us
    pallas_call x1, Pallas kernels: 152 us -> 126 us  [mega(): pl.pallas_call(kernel, out_shape=(S((8, 4096, 128), BF), S((128, 4096), B...]
    dot_general x3 -> x0, matrix products: 9.36 us -> none  [the longest x1 6.26 us: shards(): lax.dot_general(dq, wq_all, (((0, 2), (0, 2)), ((), ())), preferred_eleme...]
    sub x2 -> x0, other arithmetic: 3.15 us -> none  [norm_back(): return factor * weighted - widened * factor * factor * factor * inner]
    unnamed x14 -> x4, local copies, waits for them, and re-layouts: 1.94 us -> 3.59 us
where the time goes in v2:
time: 133 us
  Pallas kernels  126 us (95%)
  local copies, waits for them, and re-layouts  3.59 us (3%)
  other arithmetic  2.91 us (2%)
    pallas_call x1, Pallas kernels, mega(): pl.pallas_call(kernel, out_shape=(S((8, 4096, 128), BF), S((128, 4096), B...  126 us
    unnamed x4, local copies, waits for them, and re-layouts  3.59 us
    convert_element_type x1, other arithmetic, shards(): return (grad_target, grad_source, grad_out_proj.astype(F32))  2.91 us

profile of v2, /device:TPU:1, one launch (start us, length us, event | category | flops | bytes accessed | tf_op | source)
XLA Modules:
  0.0 132.8 jit_solution(15463936325741834949)
XLA Ops:
  0.6 125.7 %shard_map.112 = (bf16[8,4096,128]{2,1,0:T(8,128)(2,1)}, bf16[128,4096]{1,0:T(8,128)(2,1)}, f32[64,4096]{1,0:T(8,128)}, f32[128,4096]{1,0:T(8,128)}) custom-call(bf16[64,4096]{1,0:T(8,128)(2,1)} %tgt.1, bf16[128,4096]{1,0:T(8,128)(2,1)} %src.1, f32[1,4096]{1,0:T(1,128)} %bitcast.2, f32[1,4096]{1,0:T(1,128)} %bitcast.3, bf16[4096,128]{1,0:T(8,128)(2,1)} %wq.1, ...), custom_call_target="tpu_custom_call" | custom-call | tf_op jit(solution)/shard_map/pallas_call | solution.py:693
  126.3 0.0 copy-start
  126.3 2.9 %convert_element_type.3 = f32[128,4096]{1,0:T(8,128)} convert(bf16[128,4096]{1,0:T(8,128)(2,1)} %get-tuple-element.8) | non-fusion elementwise | flops 524288 | bytes 3145728 | tf_op jit(solution)/shard_map/convert_element_type | solution.py:727
  129.2 2.3 %copy.14 = f32[64,4096]{1,0:T(8,128)} copy(f32[64,4096]{1,0:T(8,128)} %get-tuple-element.12) | data formatting | bytes 2097152
  131.5 0.0 copy-done
  131.5 1.3 copy.15
Async XLA Ops:
  126.3 5.2 %copy-start = (f32[128,4096]{1,0:T(8,128)S(1)}, f32[128,4096]{1,0:T(8,128)}, u32[]{:S(2)}) copy-start(f32[128,4096]{1,0:T(8,128)} %get-tuple-element.13) | copy-start | bytes 6291460
